TPU v7x, 32 devices: a whole 2x2x4 slice. The times are simulated.
32 devices in a mesh: kv: 8 (over z, x), tp: 4 (over y, core).
Axes of the slice: x: 2, y: 2, z: 4, core: 2. Of those that a mesh axis runs over, the one named last changes fastest.
Arguments:
- activations: bfloat16 [384, 2048], P(None, ('kv', 'tp')), may hold values from -6 to 6
- latent_cache: bfloat16 [24, 16384, 288], P(None, 'kv'), may hold values from -6 to 6
- lengths: int32 [24], replicated, may hold values from 4096 to 16352, as said below
- accepted: int32 [24], replicated, may hold values from 0 to 16
- parents: int32 [24, 16], replicated, may hold values from -1 to 14, as said below
- w_query_down: bfloat16 [2048, 512], P(('kv', 'tp')), may hold values from -0.125 to 0.125
- w_key_down: bfloat16 [2048, 288], P(('kv', 'tp')), may hold values from -0.125 to 0.125
- gain_input: bfloat16 [2048], P(('kv', 'tp')), may hold values from 0.099609375 to 1.8984375
- gain_query: bfloat16 [512], replicated, may hold values from 0.099609375 to 1.8984375
- gain_key: bfloat16 [256], replicated, may hold values from 0.099609375 to 1.8984375
- w_query: bfloat16 [512, 16, 288], P(None, 'tp'), as said below
- w_value: bfloat16 [16, 256, 64], replicated, may hold values from -0.375 to 0.375
- w_out: bfloat16 [1024, 2048], P('tp', 'kv'), may hold values from -1 to 1, as said below
- gain_output: bfloat16 [2048], P('kv'), may hold values from 0.099609375 to 1.8984375
Outputs:
- mixed: bfloat16 [384, 2048], P(None, 'kv')
- new_cache: bfloat16 [24, 16384, 288], P(None, 'kv')
Inputs may be any that keep to these rules, and one draw needn't show every extreme that they name: One sequence has lengths exactly 16352 and another exactly 4096; which ones varies. accepted is between 0 and 16, so the proposals' positions lie below 16384. `parents`: the parent of proposal i is -1 or a proposal with a smaller index; proposal 0 has parent -1; the proposals of exactly one sequence (which one varies) form a single chain; the other sequences' proposals form general trees. `w_query`: entries are normal with standard deviation (1536)^(-1/2) cut at six standard deviations; in the hidden draw the heads whose index is a multiple of 4 are 48 times larger. `w_out`: entries of order (1024)^(-1/2).
All inputs are finite; a program needn't handle non-finite values.
Results may differ from a plain program's by a relative error of at most 0.0096.
The roundings to bfloat16 on the way count: a program that leaves them out, or rounds other values in their place, can miss the bound.
Values may be sent and summed in bfloat16 or wider, within the bound.
A program may use at most 192 MiB of HBM per device.

v0:
```python
import jax
import jax.numpy as jnp
from jax import lax
from jax.sharding import PartitionSpec as P

D = 2048
ROPE_DIM = 32
NOPE_DIM = 64
epsilon = 1e-06
rope_base = 10000.0
score_after_mask = -1e30


def rotate(component, places):
    half_width = component.shape[-1] // 2
    frequency = rope_base ** (-jnp.arange(half_width, dtype=jnp.float32) / half_width)
    angles = places.astype(jnp.float32)[:, None] * frequency[None, :]
    target_shape = (places.shape[0],) + (1,) * (component.ndim - 2) + (half_width,)
    cosine = jnp.cos(angles).reshape(target_shape)
    sine_part = jnp.sin(angles).reshape(target_shape)
    front_half = component[..., :half_width]
    back_half = component[..., half_width:]
    return jnp.concatenate(
        [front_half * cosine - back_half * sine_part, back_half * cosine + front_half * sine_part],
        axis=-1,
    )


def normalize(values, scales):
    return (
        values
        * lax.rsqrt(jnp.mean(values * values, axis=-1, keepdims=True) + epsilon)
        * scales.astype(jnp.float32)
    )


def ancestry(parents):
    seq_count, prop_count = parents.shape
    slot_ids = jnp.arange(prop_count, dtype=jnp.int32)
    parent_links = (parents[:, :, None] == slot_ids[None, None, :]).astype(jnp.float32)
    identity = jnp.broadcast_to(jnp.eye(prop_count, dtype=jnp.float32), parent_links.shape)
    reached = jnp.minimum(identity + parent_links, 1.0)
    for repeat in range((prop_count - 1).bit_length()):
        reached = jnp.minimum(
            jnp.einsum("sij,sjk->sik", reached, reached, precision=lax.Precision.HIGHEST), 1.0
        )
    depths = (jnp.sum(reached, axis=-1) - 1.0).astype(jnp.int32)
    return (reached, depths)


def down_terms(features, gain_rows, query_down, key_down):
    as_float = features.astype(jnp.float32)
    scaled = (as_float * gain_rows.astype(jnp.float32)).astype(jnp.bfloat16)
    squares = jnp.sum(as_float * as_float, axis=-1)
    query_segment = jnp.dot(scaled, query_down, preferred_element_type=jnp.float32)
    key_segment = jnp.dot(scaled, key_down, preferred_element_type=jnp.float32)
    return (squares, query_segment, key_segment)


def partial_attend(queries, key_rows, slot_index, onehot, reached, kv_rank, value_locally):
    score_scale = (NOPE_DIM + ROPE_DIM) ** (-0.5)
    ancestors = jnp.einsum("sij,snj->sin", reached, onehot, precision=lax.Precision.HIGHEST)
    visible = ((slot_index < 0)[:, None, :] | (ancestors > 0.5))[:, :, None, :]
    scores = (
        jnp.einsum("siha,sna->sihn", queries, key_rows, preferred_element_type=jnp.float32)
        * score_scale
    )
    masked = jnp.where(visible, scores, score_after_mask)
    maxima = jnp.max(masked, axis=-1)
    weights = jnp.where(visible, jnp.exp(masked - maxima[..., None]), 0.0)
    totals = jnp.sum(weights, axis=-1)
    weighted = jnp.einsum(
        "sihn,snk->sihk",
        weights.astype(jnp.bfloat16),
        key_rows[:, :, :kv_rank],
        preferred_element_type=jnp.float32,
    )
    value_fraction = (weighted / jnp.maximum(totals, 1.0)[..., None]).astype(jnp.bfloat16)
    values = jnp.einsum(
        "pwmb,mbe->pwme", value_fraction, value_locally, preferred_element_type=jnp.float32
    )
    return (maxima, totals, values.astype(jnp.bfloat16))


def combine_parts(maxima, totals, values):
    largest = jnp.max(maxima, axis=0)
    shares = totals * jnp.exp(maxima - largest[None])
    summed = jnp.sum(shares[..., None] * values.astype(jnp.float32), axis=0)
    return (summed / jnp.sum(shares, axis=0)[..., None]).astype(jnp.bfloat16)


def local(
    activations,
    latent_cache,
    lengths,
    accepted,
    parents,
    w_query_down,
    w_key_down,
    gain_input,
    gain_query,
    gain_key,
    w_query,
    w_value,
    w_out,
    gain_output,
):
    seq_count, prop_count = parents.shape
    row_count = activations.shape[0]
    heads_here = w_query.shape[1]
    kv_rank = gain_key.shape[0]
    span_len = latent_cache.shape[1]
    reached, depths = ancestry(parents)
    filled = lengths + accepted
    places = (filled[:, None] + depths).reshape(-1)
    features, gain_rows, query_down, key_down = (
        lax.all_gather(activations, "tp", axis=1, tiled=True),
        lax.all_gather(gain_input, "tp", axis=0, tiled=True),
        lax.all_gather(w_query_down, "tp", axis=0, tiled=True),
        lax.all_gather(w_key_down, "tp", axis=0, tiled=True),
    )
    squares, query_segment, key_segment = down_terms(features, gain_rows, query_down, key_down)
    squares, query_raw, key_raw = lax.psum((squares, query_segment, key_segment), "kv")
    inverse = lax.rsqrt(squares / D + epsilon)[:, None]
    query_low = normalize(query_raw * inverse, gain_query).astype(jnp.bfloat16)
    key_full = key_raw * inverse
    mapped_output = jnp.dot(
        query_low, w_query.reshape(w_query.shape[0], -1), preferred_element_type=jnp.float32
    )
    mapped_output = mapped_output.reshape(row_count, heads_here, -1)
    queries = jnp.concatenate(
        [mapped_output[..., :kv_rank], rotate(mapped_output[..., kv_rank:], places)], axis=-1
    ).astype(jnp.bfloat16)
    fresh_rows = jnp.concatenate(
        [normalize(key_full[:, :kv_rank], gain_key), rotate(key_full[:, kv_rank:], places)], axis=-1
    ).astype(jnp.bfloat16)
    locations_held = lax.axis_index("kv") * span_len + jnp.arange(span_len, dtype=jnp.int32)
    slot_index = locations_held[None, :] - filled[:, None]
    onehot = slot_index[:, :, None] == jnp.arange(prop_count, dtype=jnp.int32)[None, None, :]
    fresh_block = fresh_rows.reshape(seq_count, prop_count, -1)
    placed = jnp.einsum(
        "snj,sja->sna", onehot.astype(jnp.bfloat16), fresh_block, preferred_element_type=jnp.float32
    ).astype(jnp.bfloat16)
    updated = jnp.where(jnp.any(onehot, axis=-1)[:, :, None], placed, latent_cache)
    head_start = lax.axis_index("tp") * heads_here
    value_locally = lax.dynamic_slice_in_dim(w_value, head_start, heads_here, 0)
    maxima, totals, values = partial_attend(
        queries.reshape(seq_count, prop_count, heads_here, -1),
        updated,
        slot_index,
        onehot.astype(jnp.float32),
        reached,
        kv_rank,
        value_locally,
    )
    maxima = maxima.reshape(1, row_count, heads_here)
    totals = totals.reshape(1, row_count, heads_here)
    values = values.reshape(1, row_count, heads_here, -1)
    maxima, totals = (
        lax.all_gather(maxima, "kv", axis=0, tiled=True),
        lax.all_gather(totals, "kv", axis=0, tiled=True),
    )
    values = lax.all_gather(values, "kv", axis=0, tiled=True)
    attended = combine_parts(maxima, totals, values).reshape(row_count, -1)
    head_terms = jnp.dot(attended, w_out, preferred_element_type=jnp.float32)
    mixed_raw = lax.psum(head_terms, "tp")
    total_sq = lax.psum(jnp.sum(mixed_raw * mixed_raw, axis=-1), "kv")
    result = (
        mixed_raw * lax.rsqrt(total_sq / D + epsilon)[:, None] * gain_output.astype(jnp.float32)
    ).astype(jnp.bfloat16)
    return (result, updated)


def solution(mesh):
    in_specs = (
        P(None, ("kv", "tp")),
        P(None, "kv", None),
        P(),
        P(),
        P(),
        P(("kv", "tp"), None),
        P(("kv", "tp"), None),
        P(("kv", "tp")),
        P(),
        P(),
        P(None, "tp", None),
        P(),
        P("tp", "kv"),
        P("kv"),
    )
    out_specs = (P(None, "kv"), P(None, "kv", None))
    return jax.shard_map(local, mesh=mesh, in_specs=in_specs, out_specs=out_specs, check_vma=False)
```

profile of v0, /device:TPU:0, one launch (start us, length us, event | category | flops | bytes accessed | tf_op | source)
XLA Modules:
  0.0 322.6 jit_solution(7853236697493390630)
XLA Ops:
  7.2 1.3 dynamic-slice
  9.2 0.9 dynamic-update-slice
  10.1 8.4 %all-reduce = bf16[256]{0:T(256)(128)(2,1)S(1)} all-reduce(bf16[256]{0:T(256)(128)(2,1)S(1)} %dynamic-update-slice), channel_id=1, replica_groups=mesh['kv'=8,'tp'=4] {'tp'}, use_global_device_ids=true, to_apply=%add | all-reduce | flops 256 | bytes 1024
  18.5 5.8 %all_gather.21 = bf16[384,256]{0,1:T(8,128)(2,1)S(1)} all-gather(bf16[384,64]{0,1:T(8,128)(2,1)} %param.14), channel_id=1, replica_groups=mesh['kv'=8,'tp'=4] {'tp'}, dimensions={1}, use_global_device_ids=true | all-gather | bytes 245760 | tf_op jit(solution)/shard_map/all_gather | solution.py:117
  24.3 6.0 %all_gather.23 = bf16[256,512]{1,0:T(8,128)(2,1)S(1)} all-gather(bf16[64,512]{1,0:T(8,128)(2,1)} %param.19), channel_id=1, replica_groups=mesh['kv'=8,'tp'=4] {'tp'}, dimensions={0}, use_global_device_ids=true | all-gather | bytes 327680 | tf_op jit(solution)/shard_map/all_gather | solution.py:119
  30.3 5.8 %all_gather.24 = bf16[256,288]{1,0:T(8,128)(2,1)S(1)} all-gather(bf16[64,288]{1,0:T(8,128)(2,1)} %param.20), channel_id=1, replica_groups=mesh['kv'=8,'tp'=4] {'tp'}, dimensions={0}, use_global_device_ids=true | all-gather | bytes 184320 | tf_op jit(solution)/shard_map/all_gather | solution.py:120
  36.1 1.3 fusion.49
  37.4 1.1 fusion.47
  38.6 22.2 %psum.36 = f32[384]{0:T(512)S(1)} all-reduce(f32[384]{0:T(512)S(1)} %fusion.28), channel_id=1, replica_groups=mesh['kv'=8,'tp'=4] {'kv'}, use_global_device_ids=true, to_apply=%region_2.0 | all-reduce | flops 384 | bytes 3072 | tf_op jit(solution)/shard_map/psum | solution.py:123
  61.5 0.8 copy.38
  65.4 1.5 fusion.12
  67.0 2.0 compare_or_fusion
  69.1 51.6 %all-reduce.7.cloned.1.call-done = (f32[384,288]{0,1:T(8,128)}, f32[384,512]{1,0:T(8,128)}) async-done(((f32[384,288]{0,1:T(8,128)}, f32[384,512]{1,0:T(8,128)}), (f32[384,288]{0,1:T(8,128)}, f32[384,512]{1,0:T(8,128)})) %all-reduce.7.cloned.1.call-update) | async-done | bytes 1228816 | tf_op jit(solution)/shard_map/psum | solution.py:123
  120.7 1.0 broadcast_multiply_fusion
  122.2 0.7 copy.61
  123.0 0.7 copy.62
  123.7 1.4 multiply_reduce_fusion.1
  125.1 2.0 fusion.22
  128.9 25.2 %convert_select_fusion = bf16[24,2048,288]{1,2,0:T(8,128)(2,1)} fusion(bf16[24,2048,288]{1,2,0:T(8,128)(2,1)} %param.15, pred[24,2048]{1,0:T(8,128)(4,1)} %fusion.12, s32[24,2048]{1,0:T(8,128)S(1)} %broadcast_subtract_fusion, bf16[24,16,16]{2,1,0:T(8,128)(2,1)} %bitcast.62, bf16[24,16,16]{2,1,0:T(8,128)(2,1)} %bitcast.61, bf16[24,16,256]{2,1,0:T(8,128)(2,1)S(1)} %bitcast.60), kind=kOutput, calls=%fused_computation.2 | convolution fusion | flops 482746368 | bytes 57090048 | tf_op jit(solution)/shard_map/snj,sja->sna/dot_general | solution.py:141
  154.1 15.5 %fusion.3 = (f32[24,16,4]{1,2,0:T(4,128)S(1)}, f32[24,16,4,2048]{3,1,2,0:T(8,128)}) fusion(pred[24,16,2048]{2,1,0:T(8,128)(4,1)S(1)} %compare_or_fusion, bf16[24,2048,288]{1,2,0:T(8,128)(2,1)} %convert_select_fusion, bf16[24,16,4,16]{3,1,2,0:T(8,128)(2,1)S(1)} %copy.44, bf16[24,16,4,16]{3,1,2,0:T(8,128)(2,1)S(1)} %copy.43, ...), kind=kOutput, calls=%fused_computation.7 | convolution fusion | flops 1824029184 | bytes 42571776 | tf_op jit(solution)/shard_map/siha,sna->sihn/dot_general | solution.py:65
  169.6 6.9 %fusion.5 = f32[24,16,4]{1,2,0:T(4,128)S(1)} fusion(f32[24,16,4,2048]{3,1,2,0:T(8,128)} %get-tuple-element.17, f32[24,16,4]{1,2,0:T(4,128)S(1)} %get-tuple-element.16, pred[24,16,2048]{2,1,0:T(8,128)(4,1)S(1)} %compare_or_fusion), kind=kLoop, calls=%fused_computation.9 | loop fusion | flops 15727104 | bytes 13381632 | tf_op jit(solution)/shard_map/reduce_sum | solution.py:71
  176.5 15.1 %divide_convert_fusion = bf16[24,16,4,256]{3,1,2,0:T(8,128)(2,1)S(1)} fusion(bf16[24,2048,288]{1,2,0:T(8,128)(2,1)} %convert_select_fusion, f32[24,16,4,2048]{3,1,2,0:T(8,128)} %get-tuple-element.17, f32[24,16,4]{1,2,0:T(4,128)S(1)} %get-tuple-element.16, pred[24,16,2048]{2,1,0:T(8,128)(4,1)S(1)} %compare_or_fusion, f32[24,16,4]{1,2,0:T(4,128)S(1)} %broadcast_maximum_fusion), kind=kOutput, calls=%fused_computation.21 | convolution fusion | flops 1627127808 | bytes 39333888 | tf_op jit(solution)/shard_map/sihn,snk->sihk/dot_general | solution.py:72
  191.7 1.6 fusion.16
  193.4 0.8 copy.53
  194.5 30.7 %all_gather.26 = f32[8,384,4]{1,2,0:T(4,128)S(1)} all-gather(f32[1,384,4]{1,2,0:T(4,128)S(1)} %reshape.200), channel_id=1, replica_groups=mesh['kv'=8,'tp'=4] {'kv'}, dimensions={0}, use_global_device_ids=true | all-gather | bytes 55296 | tf_op jit(solution)/shard_map/all_gather | solution.py:160
  225.3 30.9 %all_gather.25 = f32[8,384,4]{1,2,0:T(4,128)S(1)} all-gather(f32[1,384,4]{1,2,0:T(4,128)S(1)} %reshape.199), channel_id=1, replica_groups=mesh['kv'=8,'tp'=4] {'kv'}, dimensions={0}, use_global_device_ids=true | all-gather | bytes 55296 | tf_op jit(solution)/shard_map/all_gather | solution.py:161
  256.2 1.8 multiply_reduce_fusion
  258.7 1.0 fusion.61
  259.8 32.0 %all-reduce.5.cloned.1.call-done = f32[384,256]{1,0:T(8,128)} async-done(((f32[384,256]{1,0:T(8,128)}), f32[384,256]{1,0:T(8,128)}) %all-reduce.5.cloned.1.call-update) | async-done | bytes 393232 | tf_op jit(solution)/shard_map/psum | solution.py:166
  291.7 1.1 multiply_reduce_fusion.2
  292.9 21.4 %psum.39 = f32[384]{0:T(512)S(1)} all-reduce(f32[384]{0:T(512)S(1)} %multiply_reduce_fusion.2), channel_id=1, replica_groups=mesh['kv'=8,'tp'=4] {'kv'}, use_global_device_ids=true, to_apply=%region_15.16 | all-reduce | flops 384 | bytes 3072 | tf_op jit(solution)/shard_map/psum | solution.py:167
  314.2 1.8 multiply_convert_fusion.1
  (59 shorter events, 7.4 us)
Async XLA Ops:
  7.2 117.9 %copy-start = (bf16[512,4,288]{0,2,1:T(8,128)(2,1)S(1)}, bf16[512,4,288]{0,2,1:T(8,128)(2,1)}, u32[]{:S(2)}) copy-start(bf16[512,4,288]{0,2,1:T(8,128)(2,1)} %param.24) | copy-start | bytes 3538948
  7.2 113.5 %all-reduce.7.cloned.1.call-start = ((), (), s32[]{:S(2)}) async-start(), calls=%async_computation.2 | async-start | bytes 2457600 | tf_op jit(solution)/shard_map/psum | solution.py:123
  38.5 217.7 %all-gather.2.cloned.1.call-start = ((), (), s32[]{:S(2)}) async-start(), calls=%async_computation | async-start | bytes 1769472 | tf_op jit(solution)/shard_map/all_gather | solution.py:163
  176.5 82.2 %copy-start.2 = (bf16[256,256]{1,0:T(8,128)(2,1)S(1)}, bf16[256,256]{1,0:T(8,128)(2,1)}, u32[]{:S(2)}) copy-start(bf16[256,256]{1,0:T(8,128)(2,1)} %param.26) | copy-start | bytes 393220
  176.5 83.2 %copy-start.3 = (bf16[256]{0:T(256)(128)(2,1)S(1)}, bf16[256]{0:T(256)(128)(2,1)}, u32[]{:S(2)}) copy-start(bf16[256]{0:T(256)(128)(2,1)} %param.27) | copy-start | bytes 1540
  176.5 139.5 %copy-start.1 = (bf16[512,4,288]{0,2,1:T(8,128)(2,1)S(1)}, bf16[512,4,288]{0,2,1:T(8,128)(2,1)}, u32[]{:S(2)}) copy-start(bf16[512,4,288]{0,2,1:T(8,128)(2,1)} %param.24) | copy-start | bytes 3538948
  194.2 97.5 %all-reduce.5.cloned.1.call-start = ((), (), s32[]{:S(2)}) async-start(), calls=%async_computation.1 | async-start | bytes 786432 | tf_op jit(solution)/shard_map/psum | solution.py:166
Sparse Core Ops, SparseCore 0:
  38.6 81.9 all-reduce.6
  194.4 43.4 all-gather.1
  259.9 31.8 all-reduce.4
where the time goes:
time: 323 us
  blocking collectives  131 us (41%)
  waiting for transfers between devices  83.6 us (26%)
  matrix products  66.4 us (21%)
  other arithmetic  18.6 us (6%)
  between operations  14.7 us (5%)
  local copies, waits for them, and re-layouts  7.89 us (2%)
    psum x1, waiting for transfers between devices, local(): lax.psum((squares, query_segment, key_segment), 'kv')  51.6 us
    psum x1, waiting for transfers between devices, local(): mixed_raw = lax.psum(head_terms, 'tp')  32 us
    all_gather x1, blocking collectives, local(): lax.all_gather(totals, 'kv', axis=0, tiled=True)  30.9 us
    all_gather x1, blocking collectives, local(): lax.all_gather(maxima, 'kv', axis=0, tiled=True)  30.7 us
    dot_general x1, matrix products, local(): jnp.einsum('snj,sja->sna', onehot.astype(jnp.bfloat16), fresh_block, pref...  25.2 us
    psum x1, blocking collectives, local(): lax.psum((squares, query_segment, key_segment), 'kv')  22.2 us
    psum x1, blocking collectives, local(): total_sq = lax.psum(jnp.sum(mixed_raw * mixed_raw, axis=-1), 'kv')  21.4 us
    dot_general x1, matrix products, partial_attend(): jnp.einsum('siha,sna->sihn', queries, key_rows, preferred_element_type=jn...  15.5 us
  transfers between devices with their start and end apart: 3, of which 2 were waited for; matrix products, arithmetic and copies ran while one was open for 3% of the time, Pallas kernels for 0%

commit v1 on v0

--- a/solution.py
+++ b/solution.py
@@ -156,8 +156,14 @@
     maxima = maxima.reshape(1, row_count, heads_here)
     totals = totals.reshape(1, row_count, heads_here)
     values = values.reshape(1, row_count, heads_here, -1)
+
+    def deliver_the_sectors(slab_in, comm_axis):
+        response = jnp.stack([slab_in for _ in range(lax.axis_size(comm_axis))])
+        even = lax.all_to_all(response, axis_name=comm_axis, split_axis=0, concat_axis=0)
+        return jnp.concatenate(even, axis=0)
+
     maxima, totals = (
-        lax.all_gather(maxima, "kv", axis=0, tiled=True),
+        deliver_the_sectors(maxima, "kv"),
         lax.all_gather(totals, "kv", axis=0, tiled=True),
     )
     values = lax.all_gather(values, "kv", axis=0, tiled=True)

time: 323 us -> 304 us (0.941)
  blocking collectives: 131 us -> 101 us
  waiting for transfers between devices: 83.6 us -> 90.3 us
  starting transfers between devices: 0.12 us -> 3.73 us
    all_gather x1 -> x0, blocking collectives: 30.7 us -> none  [local(): lax.all_gather(maxima, 'kv', axis=0, tiled=True)]
    all_gather x1, waiting for transfers between devices: 0.02 us -> 7.29 us  [local(): values = lax.all_gather(values, 'kv', axis=0, tiled=True)]
    all_to_all x0 -> x1, starting transfers between devices: none -> 3.62 us  [deliver_the_sectors(): lax.all_to_all(response, axis_name=comm_axis, split_axis=0, concat_axis=0)]
  transfers between devices with their start and end apart: 3 -> 4, of which waited for: 2 -> 3; matrix products, arithmetic and copies ran while one was open for 3% -> 3% of each run, Pallas kernels for 0% -> 0%
where the time goes in v1:
time: 304 us; the launch traced here: 303 us
  blocking collectives  101 us (33%)
  waiting for transfers between devices  90.3 us (30%)
  matrix products  66.4 us (22%)
  other arithmetic  18.6 us (6%)
  between operations  14.7 us (5%)
  local copies, waits for them, and re-layouts  8.52 us (3%)
  starting transfers between devices  3.73 us (1%)
    psum x1, waiting for transfers between devices, local(): lax.psum((squares, query_segment, key_segment), 'kv')  51.6 us
    all_gather x1, blocking collectives, local(): lax.all_gather(totals, 'kv', axis=0, tiled=True)  31.7 us
    psum x1, waiting for transfers between devices, local(): mixed_raw = lax.psum(head_terms, 'tp')  31.3 us
    dot_general x1, matrix products, local(): jnp.einsum('snj,sja->sna', onehot.astype(jnp.bfloat16), fresh_block, pref...  25.2 us
    psum x1, blocking collectives, local(): lax.psum((squares, query_segment, key_segment), 'kv')  22.2 us
    psum x1, blocking collectives, local(): total_sq = lax.psum(jnp.sum(mixed_raw * mixed_raw, axis=-1), 'kv')  21.4 us
    dot_general x1, matrix products, partial_attend(): jnp.einsum('siha,sna->sihn', queries, key_rows, preferred_element_type=jn...  15.5 us
    dot_general x1, matrix products, partial_attend(): jnp.einsum('sihn,snk->sihk', weights.astype(jnp.bfloat16), key_rows[:, :,...  15.1 us
  transfers between devices with their start and end apart: 4, of which 3 were waited for; matrix products, arithmetic and copies ran while one was open for 3% of the time, Pallas kernels for 0%

profile of v1, /device:TPU:0, one launch (start us, length us, event | category | flops | bytes accessed | tf_op | source)
XLA Modules:
  0.0 303.5 jit_solution(15356109101237173642)
XLA Ops:
  7.2 1.3 dynamic-slice
  9.2 0.9 dynamic-update-slice
  10.1 8.4 %all-reduce = bf16[256]{0:T(256)(128)(2,1)S(1)} all-reduce(bf16[256]{0:T(256)(128)(2,1)S(1)} %dynamic-update-slice), channel_id=1, replica_groups=mesh['kv'=8,'tp'=4] {'tp'}, use_global_device_ids=true, to_apply=%add | all-reduce | flops 256 | bytes 1024
  18.5 5.8 %all_gather.18 = bf16[384,256]{0,1:T(8,128)(2,1)S(1)} all-gather(bf16[384,64]{0,1:T(8,128)(2,1)} %param.14), channel_id=1, replica_groups=mesh['kv'=8,'tp'=4] {'tp'}, dimensions={1}, use_global_device_ids=true | all-gather | bytes 245760 | tf_op jit(solution)/shard_map/all_gather | solution.py:117
  24.3 6.0 %all_gather.20 = bf16[256,512]{1,0:T(8,128)(2,1)S(1)} all-gather(bf16[64,512]{1,0:T(8,128)(2,1)} %param.19), channel_id=1, replica_groups=mesh['kv'=8,'tp'=4] {'tp'}, dimensions={0}, use_global_device_ids=true | all-gather | bytes 327680 | tf_op jit(solution)/shard_map/all_gather | solution.py:119
  30.3 5.8 %all_gather.21 = bf16[256,288]{1,0:T(8,128)(2,1)S(1)} all-gather(bf16[64,288]{1,0:T(8,128)(2,1)} %param.20), channel_id=1, replica_groups=mesh['kv'=8,'tp'=4] {'tp'}, dimensions={0}, use_global_device_ids=true | all-gather | bytes 184320 | tf_op jit(solution)/shard_map/all_gather | solution.py:120
  36.1 1.3 fusion.49
  37.4 1.1 fusion.47
  38.6 22.2 %psum.36 = f32[384]{0:T(512)S(1)} all-reduce(f32[384]{0:T(512)S(1)} %fusion.28), channel_id=1, replica_groups=mesh['kv'=8,'tp'=4] {'kv'}, use_global_device_ids=true, to_apply=%region_2.0 | all-reduce | flops 384 | bytes 3072 | tf_op jit(solution)/shard_map/psum | solution.py:123
  61.5 0.8 copy.38
  65.4 1.5 fusion.12
  67.0 2.0 compare_or_fusion
  69.1 51.6 %all-reduce.7.cloned.1.call-done = (f32[384,288]{0,1:T(8,128)}, f32[384,512]{1,0:T(8,128)}) async-done(((f32[384,288]{0,1:T(8,128)}, f32[384,512]{1,0:T(8,128)}), (f32[384,288]{0,1:T(8,128)}, f32[384,512]{1,0:T(8,128)})) %all-reduce.7.cloned.1.call-update) | async-done | bytes 1228816 | tf_op jit(solution)/shard_map/psum | solution.py:123
  120.7 1.0 broadcast_multiply_fusion
  123.0 0.7 copy.62
  123.7 1.4 multiply_reduce_fusion.1
  125.1 2.0 fusion.22
  128.9 25.2 %convert_select_fusion = bf16[24,2048,288]{1,2,0:T(8,128)(2,1)} fusion(bf16[24,2048,288]{1,2,0:T(8,128)(2,1)} %param.15, pred[24,2048]{1,0:T(8,128)(4,1)} %fusion.12, s32[24,2048]{1,0:T(8,128)S(1)} %broadcast_subtract_fusion, bf16[24,16,16]{2,1,0:T(8,128)(2,1)} %bitcast.69, bf16[24,16,16]{2,1,0:T(8,128)(2,1)} %bitcast.68, bf16[24,16,256]{2,1,0:T(8,128)(2,1)S(1)} %bitcast.67), kind=kOutput, calls=%fused_computation.2 | convolution fusion | flops 482746368 | bytes 57090048 | tf_op jit(solution)/shard_map/snj,sja->sna/dot_general | solution.py:141
  154.1 15.5 %fusion.3 = (f32[24,16,4]{1,2,0:T(4,128)S(1)}, f32[24,16,4,2048]{3,1,2,0:T(8,128)}) fusion(pred[24,16,2048]{2,1,0:T(8,128)(4,1)S(1)} %compare_or_fusion, bf16[24,2048,288]{1,2,0:T(8,128)(2,1)} %convert_select_fusion, bf16[24,16,4,16]{3,1,2,0:T(8,128)(2,1)S(1)} %copy.44, bf16[24,16,4,16]{3,1,2,0:T(8,128)(2,1)S(1)} %copy.43, ...), kind=kOutput, calls=%fused_computation.7 | convolution fusion | flops 1824029184 | bytes 42571776 | tf_op jit(solution)/shard_map/siha,sna->sihn/dot_general | solution.py:65
  169.6 6.9 %fusion.5 = f32[24,16,4]{1,2,0:T(4,128)S(1)} fusion(f32[24,16,4,2048]{3,1,2,0:T(8,128)} %get-tuple-element.17, f32[24,16,4]{1,2,0:T(4,128)S(1)} %get-tuple-element.16, pred[24,16,2048]{2,1,0:T(8,128)(4,1)S(1)} %compare_or_fusion), kind=kLoop, calls=%fused_computation.9 | loop fusion | flops 15727104 | bytes 13381632 | tf_op jit(solution)/shard_map/reduce_sum | solution.py:71
  176.5 15.1 %divide_convert_fusion = bf16[24,16,4,256]{3,1,2,0:T(8,128)(2,1)S(1)} fusion(bf16[24,2048,288]{1,2,0:T(8,128)(2,1)} %convert_select_fusion, f32[24,16,4,2048]{3,1,2,0:T(8,128)} %get-tuple-element.17, f32[24,16,4]{1,2,0:T(4,128)S(1)} %get-tuple-element.16, pred[24,16,2048]{2,1,0:T(8,128)(4,1)S(1)} %compare_or_fusion, f32[24,16,4]{1,2,0:T(4,128)S(1)} %broadcast_maximum_fusion), kind=kOutput, calls=%fused_computation.21 | convolution fusion | flops 1627127808 | bytes 39333888 | tf_op jit(solution)/shard_map/sihn,snk->sihk/dot_general | solution.py:72
  191.7 1.6 fusion.16
  193.4 0.8 copy.53
  195.0 3.6 %all-to-all-start = ((f32[8,1,384,4]{2,3,1,0:T(4,128)}), f32[8,1,384,4]{2,3,1,0:T(4,128)S(1)}, u32[]{:S(2)}, u32[]{:S(2)}) async-start(f32[8,1,384,4]{2,3,1,0:T(4,128)} %stack.3), calls=%async_computation | async-start | bytes 98304 | tf_op jit(solution)/shard_map/all_to_all | solution.py:162
  198.7 31.7 %all_gather.22 = f32[8,384,4]{1,2,0:T(4,128)S(1)} all-gather(f32[1,384,4]{1,2,0:T(4,128)S(1)} %reshape.203), channel_id=1, replica_groups=mesh['kv'=8,'tp'=4] {'kv'}, dimensions={0}, use_global_device_ids=true | all-gather | bytes 55296 | tf_op jit(solution)/shard_map/all_gather | solution.py:167
  230.4 7.3 %all-gather.2.cloned.1.call-done = bf16[8,384,4,64]{1,3,2,0:T(8,128)(2,1)} async-done(((bf16[1,384,4,64]{1,3,2,0:T(8,128)(2,1)}), bf16[8,384,4,64]{1,3,2,0:T(8,128)(2,1)}) %all-gather.2.cloned.1.call-update) | async-done | bytes 1572880 | tf_op jit(solution)/shard_map/all_gather | solution.py:169
  237.7 1.8 multiply_reduce_fusion
  240.3 1.0 fusion.64
  241.3 31.3 %all-reduce.5.cloned.1.call-done = f32[384,256]{1,0:T(8,128)} async-done(((f32[384,256]{1,0:T(8,128)}), f32[384,256]{1,0:T(8,128)}) %all-reduce.5.cloned.1.call-update) | async-done | bytes 393232 | tf_op jit(solution)/shard_map/psum | solution.py:172
  272.6 1.1 multiply_reduce_fusion.2
  273.8 21.4 %psum.39 = f32[384]{0:T(512)S(1)} all-reduce(f32[384]{0:T(512)S(1)} %multiply_reduce_fusion.2), channel_id=1, replica_groups=mesh['kv'=8,'tp'=4] {'kv'}, use_global_device_ids=true, to_apply=%region_15.16 | all-reduce | flops 384 | bytes 3072 | tf_op jit(solution)/shard_map/psum | solution.py:173
  295.1 1.8 multiply_convert_fusion.1
  (61 shorter events, 8.8 us)
Async XLA Ops:
  7.2 117.9 %copy-start = (bf16[512,4,288]{0,2,1:T(8,128)(2,1)S(1)}, bf16[512,4,288]{0,2,1:T(8,128)(2,1)}, u32[]{:S(2)}) copy-start(bf16[512,4,288]{0,2,1:T(8,128)(2,1)} %param.24) | copy-start | bytes 3538948
  7.2 113.5 %all-reduce.7.cloned.1.call-start = ((), (), s32[]{:S(2)}) async-start(), calls=%async_computation.3 | async-start | bytes 2457600 | tf_op jit(solution)/shard_map/psum | solution.py:123
  38.5 199.2 %all-gather.2.cloned.1.call-start = ((), (), s32[]{:S(2)}) async-start(), calls=%async_computation.1 | async-start | bytes 1769472 | tf_op jit(solution)/shard_map/all_gather | solution.py:169
  176.5 63.7 %copy-start.2 = (bf16[256,256]{1,0:T(8,128)(2,1)S(1)}, bf16[256,256]{1,0:T(8,128)(2,1)}, u32[]{:S(2)}) copy-start(bf16[256,256]{1,0:T(8,128)(2,1)} %param.26) | copy-start | bytes 393220
  176.5 64.8 %copy-start.3 = (bf16[256]{0:T(256)(128)(2,1)S(1)}, bf16[256]{0:T(256)(128)(2,1)}, u32[]{:S(2)}) copy-start(bf16[256]{0:T(256)(128)(2,1)} %param.27) | copy-start | bytes 1540
  176.5 120.4 %copy-start.1 = (bf16[512,4,288]{0,2,1:T(8,128)(2,1)S(1)}, bf16[512,4,288]{0,2,1:T(8,128)(2,1)}, u32[]{:S(2)}) copy-start(bf16[512,4,288]{0,2,1:T(8,128)(2,1)} %param.24) | copy-start | bytes 3538948
  195.0 35.4 %all-to-all-start = ((f32[8,1,384,4]{2,3,1,0:T(4,128)}), f32[8,1,384,4]{2,3,1,0:T(4,128)S(1)}, u32[]{:S(2)}, u32[]{:S(2)}) async-start(f32[8,1,384,4]{2,3,1,0:T(4,128)} %stack.3), calls=%async_computation | async-start | bytes 98304 | tf_op jit(solution)/shard_map/all_to_all | solution.py:162
  198.6 74.1 %all-reduce.5.cloned.1.call-start = ((), (), s32[]{:S(2)}) async-start(), calls=%async_computation.2 | async-start | bytes 786432 | tf_op jit(solution)/shard_map/psum | solution.py:172
Sparse Core Ops, SparseCore 0:
  38.6 81.9 all-reduce.6
  194.4 43.3 all-gather.1
  241.4 31.1 all-reduce.4
